TPU v7x, 768 devices: a whole 4x8x12 slice. The times are simulated.
768 devices in a mesh: row: 24 (over z, core), col: 32 (over y, x).
Axes of the slice: x: 4, y: 8, z: 12, core: 2. Of those that a mesh axis runs over, the one named last changes fastest.
Arguments:
- tokens: bfloat16 [192, 576, 2048], P('row', 'col'), may hold values from -6 to 6
- norm_gain: bfloat16 [2048], replicated, may hold values from 0.099609375 to 1.8984375
- w_in: bfloat16 [2048, 1152], replicated, may hold values from -0.125 to 0.125
- w_out: bfloat16 [1152, 2048], replicated, may hold values from -0.1875 to 0.1875
Outputs:
- mixed: bfloat16 [576, 192, 2048], P('row', 'col')
All inputs are finite; a program needn't handle non-finite values.
Results may differ from a plain program's by a relative error of at most 0.013.
Values may be sent and summed in bfloat16 or wider, within the bound.
A program may use at most 64 MiB of HBM per device.

v0:
```python
import math

import jax
import jax.numpy as jnp
import numpy as np
from jax import lax
from jax.experimental import pallas as pl
from jax.experimental.pallas import tpu as pltpu
from jax.sharding import PartitionSpec as P

MESH = pl.DeviceIdType.MESH
F32 = jnp.float32
BF16 = jnp.bfloat16
NORM_EPS = 1e-06

D, GROUP, F = 2048, 128, 1152
LEN_A, LEN_B = 192, 576
NR, NC = 24, 32
GROUPS = F // GROUP
POSITIONS = LEN_A * LEN_B


def host_tables():
    j = np.arange(GROUP)
    lane = np.arange(GROUP)
    q, ch = lane // 16, lane % 16
    m = 8 * q + ch % 8
    sine = ch >= 8
    m = np.where(sine & (m == 0), 64, m)
    sine = sine & (m != 64)
    angle = 2 * np.pi * (j[:, None] * m[None, :] % GROUP) / GROUP
    tc = np.where(sine[None, :], np.sin(angle), np.cos(angle)) / math.sqrt(GROUP)
    fold = np.zeros((GROUP, GROUP))
    fold[lane, m] = 1.0
    pair = (m != 0) & (m != 64)
    fold[lane[pair], GROUP - m[pair]] = np.where(sine[pair], -1.0, 1.0)
    a = np.arange(LEN_A)
    ma = np.zeros((NC, 6, LEN_A))
    for c in range(NC):
        for i in range(3):
            w = 2 * np.pi * (a * (3 * c + i) % LEN_A) / LEN_A
            ma[c, i] = np.cos(w)
            ma[c, 3 + i] = -np.sin(w)
    ma[0, 3] = np.cos(np.pi * a)
    ma = ma.reshape(LEN_A, LEN_A) / math.sqrt(LEN_A)
    lo, hi, r = np.meshgrid(np.arange(8), np.arange(3), np.arange(NR), indexing="ij")
    kb = (24 * r + 8 * hi + lo).reshape(-1)
    bp, cp = np.meshgrid(np.arange(18), np.arange(NC), indexing="ij")
    b = (18 * cp + bp).reshape(-1)
    parts = []
    for k in (kb, LEN_B - 1 - kb):
        w = 2 * np.pi * (k[:, None] * b[None, :] % LEN_B) / LEN_B
        parts.append(np.concatenate([np.cos(w), np.sin(w)], axis=1))
    g = np.concatenate(parts, axis=0) / math.sqrt(LEN_B)
    return [np.asarray(t, dtype=jnp.bfloat16) for t in (tc, ma, g, fold)]


TABLES = host_tables()


def swap8(x):
    lane = lax.broadcasted_iota(jnp.int32, x[0].shape, 1)
    x = list(x)
    for s in (4, 2, 1):
        shift = 16 * s
        bit = (lane & shift) != 0
        for i in range(8):
            if i & s:
                continue
            a, b = x[i], x[i + s]
            x[i] = jnp.where(bit, pltpu.roll(b, shift, 1), a)
            x[i + s] = jnp.where(bit, b, pltpu.roll(a, GROUP - shift, 1))
    return x


def peer_step(k, n):
    k = n - 2 - k
    return jnp.where(k % 2 == 0, 1 + k // 2, n - (k + 1) // 2)


def kernel(
    tok, gain, w_in, w_out, tc_h, ma_h, g_h, fold_h, out,
    xb, gn, xf, xs, wi, wo, wf, tc, ma, gg, fold, mp, tb, s1, r1, zf, s2, r2, f2,
    rr, ii, cs, sn, dd, m3, s3, r3, f3, lh, ls,
    load_sem, send1, recv1, send2, recv2, send3, recv3,
):
    row, col = lax.axis_index("row"), lax.axis_index("col")

    loads = [
        pltpu.make_async_copy(src, dst, load_sem.at[n])
        for n, (src, dst) in enumerate(
            [(tok, xb), (gain, gn), (w_in, wi), (tc_h, tc), (ma_h, ma), (fold_h, fold), (w_out, wo), (g_h, gg)]
        )
    ]
    for load in loads:
        load.start()

    barrier = pltpu.get_barrier_semaphore()

    def greet(k, carry):
        dest = lax.rem(row + 1 + k, NR)
        pl.semaphore_signal(barrier, inc=1, device_id={"row": dest}, device_id_type=MESH)
        return carry

    def greet_col(k, carry):
        dest = lax.rem(col + 1 + k, NC)
        pl.semaphore_signal(barrier, inc=1, device_id={"col": dest}, device_id_type=MESH)
        return carry

    lax.fori_loop(0, NR - 1, greet, 0)
    lax.fori_loop(0, NC - 1, greet_col, 0)

    def send_all(src, dst, ssem, rsem, axis, me, n):
        def one(k, carry):
            dest = lax.rem(me + peer_step(k, n), n)
            pltpu.make_async_remote_copy(
                src.at[dest], dst.at[me], ssem.at[dest], rsem.at[me], device_id={axis: dest}, device_id_type=MESH
            ).start()
            return carry

        lax.fori_loop(0, n - 1, one, 0)

    def wait_all(src, dst, ssem, rsem, axis, me, n, receive):
        def one(k, carry):
            peer = lax.rem(me + 1 + k, n)
            copy = pltpu.make_async_remote_copy(
                src.at[peer], dst.at[peer], ssem.at[peer], rsem.at[peer], device_id={axis: peer}, device_id_type=MESH
            )
            if receive:
                copy.wait_recv()
            else:
                copy.wait_send()
            return carry

        lax.fori_loop(0, n - 1, one, 0)

    loads[0].wait()
    loads[1].wait()

    def norm(a, carry):
        x = xb[a].astype(F32)
        y = x * lax.rsqrt(jnp.mean(x * x, axis=-1, keepdims=True) + NORM_EPS) * gn[...].astype(F32)
        for t in range(D // 128):
            xf[t, pl.ds(pl.multiple_of(24 * a, 8), 18), :] = y[:, 128 * t : 128 * (t + 1)]
        return carry

    lax.fori_loop(0, 8, norm, 0)

    def regroup(n, carry):
        for t in range(D // 128):
            y = jnp.concatenate([xf[t, pl.ds(2 * n, 8, stride=24), :], xf[t, pl.ds(2 * n + 1, 8, stride=24), :]], axis=0)
            xs[pl.ds(pl.multiple_of(16 * n, 16), 16), 128 * t : 128 * (t + 1)] = y.astype(BF16)
        return carry

    lax.fori_loop(0, 9, regroup, 0)
    loads[2].wait()
    loads[3].wait()
    mp[...] = jnp.dot(xs[...], wi[...], preferred_element_type=F32).astype(BF16)
    for g in range(GROUPS):
        values = jnp.dot(mp[:, 128 * g : 128 * (g + 1)], tc[...], preferred_element_type=F32)
        tb[g] = values.reshape(18, 8, GROUP)

    def pack(g, carry):
        o, t = g // 3, g % 3
        for hi in range(2):
            moved = swap8([tb[g, 8 * hi + n] for n in range(8)])
            for q in range(8):
                s1[8 * o + q, 2 * t + hi] = moved[q].astype(BF16)
        return carry

    lax.fori_loop(0, GROUPS, pack, 0)

    def pack_rest(o, carry):
        zero = jnp.zeros((8, GROUP), F32)
        moved = swap8([tb[3 * o + n % 4, 16 + n // 4] if n % 4 < 3 else zero for n in range(8)])
        for q in range(8):
            s1[8 * o + q, 6] = moved[q].astype(BF16)
        return carry

    lax.fori_loop(0, 3, pack_rest, 0)

    pl.semaphore_wait(barrier, NR + NC - 2)
    send_all(s1, r1, send1, recv1, "row", row, NR)
    r1[row] = s1[row]

    shape = (LEN_B, GROUP)
    line = lax.broadcasted_iota(jnp.int32, shape, 0)
    lane = lax.broadcasted_iota(jnp.int32, shape, 1)
    position = (18 * (line & 31) + (line >> 5)).astype(F32)
    sine = ((lane & 8) != 0) & jnp.logical_not((lax.rem(row, 8) == 0) & ((lane & 15) == 8))
    offset = jnp.where(sine, 0.5 * math.pi, 0.0).astype(F32)
    for tile in range(2):
        low = 3 * col + 2 * tile
        high = 3 * col + 1 if tile == 0 else jnp.where(col == 0, LEN_A // 2, 3 * col)
        frequency = jnp.where(lane < 64, low, high).astype(F32)
        angle = position * frequency * (2.0 * math.pi / POSITIONS) + offset
        cs[tile] = jnp.cos(angle)
        sn[tile] = jnp.sin(angle)
    loads[5].wait()
    loads[6].wait()

    def fold_out(g, carry):
        lines = pl.ds(pl.multiple_of(128 * g, 128), 128)
        wf[lines, :] = jnp.dot(fold[...], wo[lines, :], preferred_element_type=F32).astype(BF16)
        return carry

    lax.fori_loop(0, GROUPS, fold_out, 0)
    loads[4].wait()
    loads[7].wait()
    zf[pl.ds(7, LEN_A, stride=8), :] = jnp.zeros((LEN_A, GROUP), F32)
    for n in (54, 55):
        m3[pl.ds(n, NR, stride=56), :] = jnp.zeros((NR, GROUP), F32)

    wait_all(s1, r1, send1, recv1, "row", row, NR, True)
    arrived = jnp.concatenate([r1[:, n].astype(F32).reshape(LEN_A, GROUP) for n in range(7)], axis=1)
    turned = jnp.dot(ma[...], arrived.astype(BF16), preferred_element_type=F32)
    for n in range(7):
        zf[pl.ds(n, LEN_A, stride=8), :] = turned[:, 128 * n : 128 * (n + 1)]
    s2[...] = zf[...].reshape(NC, 48, GROUP).astype(BF16)
    send_all(s2, r2, send2, recv2, "col", col, NC)
    r2[col] = s2[col]
    wait_all(s2, r2, send2, recv2, "col", col, NC, True)

    f2[...] = r2[...].astype(F32).reshape(NC * 48, GROUP)
    inner = (col != 0).astype(F32)
    lane = lax.broadcasted_iota(jnp.int32, (NC, GROUP), 1)
    zero = jnp.zeros((NC, GROUP), F32)

    def part(i, n):
        return f2[pl.ds(8 * i + n, NC, stride=48), :]

    def sets(n):
        i0 = part(3, n)
        i0_kept = i0 * inner
        r0 = part(0, n)
        return ([r0, part(1, n), part(2, n), jnp.where(col == 0, i0, r0)], [i0_kept, part(4, n), part(5, n), i0_kept])

    for hi in range(2):
        by_t = [sets(2 * t + hi) for t in range(3)]
        for kind, target in ((0, rr), (1, ii)):
            for tile in range(2):
                x = []
                for s in (2 * tile, 2 * tile + 1):
                    x += [by_t[t][kind][s] for t in range(3)] + [zero]
                for n, moved in enumerate(swap8(x)):
                    target[tile, 32 * (8 * hi + n) : 32 * (8 * hi + n + 1), :] = moved
    last = sets(6)
    for kind, target in ((0, rr), (1, ii)):
        for tile in range(2):
            x, y = last[kind][2 * tile], last[kind][2 * tile + 1]
            target[tile, 512:544, :] = jnp.where(lane < 64, x, pltpu.roll(y, 64, 1))
            target[tile, 544:576, :] = jnp.where(lane < 64, pltpu.roll(x, 64, 1), y)
    for tile in range(2):
        at = slice(128 * tile, 128 * (tile + 1))
        dd[0:LEN_B, at] = (rr[tile] * cs[tile] + ii[tile] * sn[tile]).astype(BF16)
        dd[LEN_B : 2 * LEN_B, at] = (ii[tile] * cs[tile] - rr[tile] * sn[tile]).astype(BF16)
    lane = lax.broadcasted_iota(jnp.int32, (72, GROUP), 1)
    sine = ((lane & 8) != 0) & jnp.logical_not((lax.rem(row, 8) == 0) & ((lane & 15) == 8))
    sign = jnp.where(sine, -1.0, 1.0).astype(F32)
    for upper in range(2):
        result = jnp.dot(gg[LEN_B * upper : LEN_B * (upper + 1)], dd[...], preferred_element_type=F32)
        for tile in range(2):
            moved = swap8([result[72 * n : 72 * (n + 1), 128 * tile : 128 * (tile + 1)] for n in range(8)])
            for half in range(2):
                s = 2 * tile + half
                i = (s if s < 3 else None) if upper == 0 else (None, 4, 5, 3)[s]
                if i is None:
                    continue
                for t in range(3):
                    values = moved[4 * half + t]
                    if upper:
                        values = values * sign
                    for hi in range(3):
                        m3[pl.ds((3 * i + hi) * 3 + t, NR, stride=56), :] = values[24 * hi : 24 * (hi + 1)]
    s3[...] = m3[...].reshape(NR, 7, 8, GROUP).astype(BF16)
    send_all(s3, r3, send3, recv3, "row", row, NR)
    r3[row] = s3[row]
    wait_all(s3, r3, send3, recv3, "row", row, NR, True)

    f3[...] = r3[...].astype(F32).reshape(NR * 56, GROUP)
    for o in range(3):
        for t in range(3):
            moved = swap8([f3[pl.ds((8 * o + q) * 56 + t, 18, stride=3), :] for q in range(8)])
            for n in range(8):
                lh[3 * o + t, pl.ds(n, 18, stride=8), :] = moved[n]
    for g in range(GROUPS):
        ls[:, 128 * g : 128 * (g + 1)] = lh[g].astype(BF16)

    def project(n, carry):
        at = pl.ds(pl.multiple_of(512 * n, 512), 512)
        out[:, at] = jnp.dot(ls[...], wf[:, at], preferred_element_type=F32).astype(BF16)
        return carry

    lax.fori_loop(0, D // 512, project, 0)

    wait_all(s1, r1, send1, recv1, "row", row, NR, False)
    wait_all(s2, r2, send2, recv2, "col", col, NC, False)
    wait_all(s3, r3, send3, recv3, "row", row, NR, False)


def shards(tokens, norm_gain, w_in, w_out):
    vm = pltpu.VMEM
    dma = pltpu.SemaphoreType.DMA
    out = pl.pallas_call(
        kernel,
        out_shape=jax.ShapeDtypeStruct((144, D), BF16),
        in_specs=[pl.BlockSpec(memory_space=pl.ANY)] * 8,
        out_specs=pl.BlockSpec(memory_space=vm),
        scratch_shapes=[
            vm((8, 18, D), BF16),
            vm((1, D), BF16),
            vm((D // 128, 8 * 24, 128), F32),
            vm((144, D), BF16),
            vm((D, F), BF16),
            vm((F, D), BF16),
            vm((F, D), BF16),
            vm((GROUP, GROUP), BF16),
            vm((LEN_A, LEN_A), BF16),
            vm((2 * LEN_B, 2 * LEN_B), BF16),
            vm((GROUP, GROUP), BF16),
            vm((144, F), BF16),
            vm((GROUPS, 18, 8, GROUP), F32),
            vm((NR, 7, 8, GROUP), BF16),
            vm((NR, 7, 8, GROUP), BF16),
            vm((LEN_A * 8, GROUP), F32),
            vm((NC, 48, GROUP), BF16),
            vm((NC, 48, GROUP), BF16),
            vm((NC * 48, GROUP), F32),
            vm((2, LEN_B, GROUP), F32),
            vm((2, LEN_B, GROUP), F32),
            vm((2, LEN_B, GROUP), F32),
            vm((2, LEN_B, GROUP), F32),
            vm((2 * LEN_B, 2 * GROUP), BF16),
            vm((NR * 56, GROUP), F32),
            vm((NR, 7, 8, GROUP), BF16),
            vm((NR, 7, 8, GROUP), BF16),
            vm((NR * 56, GROUP), F32),
            vm((GROUPS, 144, GROUP), F32),
            vm((144, F), BF16),
            dma((8,)),
            dma((NR,)),
            dma((NR,)),
            dma((NC,)),
            dma((NC,)),
            dma((NR,)),
            dma((NR,)),
        ],
        compiler_params=pltpu.CompilerParams(
            collective_id=0, has_side_effects=True, vmem_limit_bytes=60 * 1024 * 1024
        ),
    )(tokens, norm_gain.reshape(1, D), w_in, w_out, *[jnp.asarray(t) for t in TABLES])
    return out.reshape(6, 3, 8, D).transpose(1, 2, 0, 3).reshape(24, 6, D)


def solution(mesh):
    in_specs = (P("row", "col", None), P(), P(), P())
    out_specs = P("row", "col", None)
    return jax.shard_map(shards, mesh=mesh, in_specs=in_specs, out_specs=out_specs, check_vma=False)
```

profile of v0, /device:TPU:1, one launch (start us, length us, event | category | flops | bytes accessed | tf_op | source)
XLA Modules:
  0.0 73.6 jit_solution(18333113031511395730)
XLA Ops:
  0.0 1.3 %reshape.9.gain = bf16[1,2048]{1,0:T(2,128)(2,1)} reshape(bf16[2048]{0:T(1024)(128)(2,1)} %param.9) | data formatting | bytes 8192 | tf_op jit(solution)/shard_map/reshape | solution.py:351
  1.3 2.3 %copy.9.tok = bf16[8,18,2048]{2,1,0:T(8,128)(2,1)} copy(bf16[8,18,2048]{2,0,1:T(8,128)(2,1)} %param.8) | data formatting | bytes 1179648 | tf_op args[0]
  3.6 68.1 %shard_map.82 = bf16[144,2048]{1,0:T(8,128)(2,1)} custom-call(bf16[8,18,2048]{2,1,0:T(8,128)(2,1)} %copy.9.tok, bf16[1,2048]{1,0:T(2,128)(2,1)} %reshape.9.gain, bf16[2048,1152]{1,0:T(8,128)(2,1)} %w_in.1, bf16[1152,2048]{1,0:T(8,128)(2,1)} %w_out.1, bf16[128,128]{1,0:T(8,128)(2,1)} %constant.8.clone.tc_h, bf16[192,192]{1,0:T(8,128)(2,1)} %constant.9.clone.ma_h, ...), custom_call_target="tpu_custom_call" | custom-call | tf_op jit(solution)/shard_map/pallas_call | solution.py:304
  71.7 1.9 %copy.11 = bf16[24,6,2048]{2,0,1:T(8,128)(2,1)} copy(bf16[24,6,2048]{2,0,1:T(8,128)(2,1)} %bitcast.5) | data formatting | bytes 1179648
where the time goes:
time: 73.9 us; the launch traced here: 73.6 us
  Pallas kernels  68.1 us (92%)
  local copies, waits for them, and re-layouts  5.51 us (7%)
    pallas_call x1, Pallas kernels, shards(): pl.pallas_call(kernel, out_shape=jax.ShapeDtypeStruct((144, D), BF16), in...  68.1 us
    unnamed x2, local copies, waits for them, and re-layouts  4.22 us

commit v1 on v0

v1 whole, which is shorter than its diff:
```python
import math

import jax
import jax.numpy as jnp
import numpy as np
from jax import lax
from jax.experimental import pallas as pl
from jax.experimental.pallas import tpu as pltpu
from jax.sharding import PartitionSpec as P

MESH = pl.DeviceIdType.MESH
F32 = jnp.float32
BF16 = jnp.bfloat16
NORM_EPS = 1e-06

D, GROUP, F = 2048, 128, 1152
LEN_A, LEN_B = 192, 576
NR, NC = 24, 32
GROUPS = F // GROUP
POSITIONS = LEN_A * LEN_B


def host_tables():
    j = np.arange(GROUP)
    lane = np.arange(GROUP)
    q, ch = lane // 16, lane % 16
    m = 8 * q + ch % 8
    sine = ch >= 8
    m = np.where(sine & (m == 0), 64, m)
    sine = sine & (m != 64)
    angle = 2 * np.pi * (j[:, None] * m[None, :] % GROUP) / GROUP
    tc = np.where(sine[None, :], np.sin(angle), np.cos(angle)) / math.sqrt(GROUP)
    fold = np.zeros((GROUP, GROUP))
    fold[lane, m] = 1.0
    pair = (m != 0) & (m != 64)
    fold[lane[pair], GROUP - m[pair]] = np.where(sine[pair], -1.0, 1.0)
    a = np.arange(LEN_A)
    ma = np.zeros((NC, 8, LEN_A))
    for c in range(NC):
        for i in range(3):
            w = 2 * np.pi * (a * (3 * c + i) % LEN_A) / LEN_A
            ma[c, i] = np.cos(w)
            ma[c, 3 + i] = -np.sin(w)
    ma[0, 3] = np.cos(np.pi * a)
    ma = ma.reshape(NC * 8, LEN_A) / math.sqrt(LEN_A)
    lo, hi, r = np.meshgrid(np.arange(8), np.arange(3), np.arange(NR), indexing="ij")
    kb = (24 * r + 8 * hi + lo).reshape(-1)
    bp, cp = np.meshgrid(np.arange(18), np.arange(NC), indexing="ij")
    b = (18 * cp + bp).reshape(-1)
    w = 2 * np.pi * (kb[:, None] * b[None, :] % LEN_B) / LEN_B
    g = np.concatenate([np.cos(w), np.sin(w)], axis=1) / math.sqrt(LEN_B)
    return [np.asarray(t, dtype=jnp.bfloat16) for t in (tc, ma, g, fold)]


TABLES = host_tables()
TILES1 = ((0, 3), (3, 5), (5, 7))
TILES3 = ((0, 2), (2, 4), (4, 7))


def swap8(x):
    lane = lax.broadcasted_iota(jnp.int32, x[0].shape, 1)
    x = list(x)
    for s in (4, 2, 1):
        shift = 16 * s
        bit = (lane & shift) != 0
        for i in range(8):
            if i & s:
                continue
            a, b = x[i], x[i + s]
            x[i] = jnp.where(bit, pltpu.roll(b, shift, 1), a)
            x[i + s] = jnp.where(bit, b, pltpu.roll(a, GROUP - shift, 1))
    return x


def peer_step(k, n):
    k = n - 2 - k
    return jnp.where(k % 2 == 0, 1 + k // 2, n - (k + 1) // 2)


def kernel(
    tok, gain, w_in, w_out, tc_h, ma_h, g_h, fold_h, out,
    xb, gn, xs, wi, wo, wf, tc, ma, gg, fold, mp, tb, s1, r1, za, zb, sa, ra, sb, rb, fa, fb,
    rr, ii, cs, sn, dd, m3, s3, r3, f3, lh, acc,
    load_sem, send1, recv1, send2, recv2, send3, recv3,
):
    row, col = lax.axis_index("row"), lax.axis_index("col")

    loads = [
        pltpu.make_async_copy(src, dst, load_sem.at[n])
        for n, (src, dst) in enumerate(
            [(tok, xb), (gain, gn), (w_in, wi), (tc_h, tc), (ma_h, ma), (fold_h, fold), (w_out, wo), (g_h, gg)]
        )
    ]
    for load in loads:
        load.start()

    barrier = pltpu.get_barrier_semaphore()

    def greet(k, carry):
        dest = lax.rem(row + 1 + k, NR)
        pl.semaphore_signal(barrier, inc=1, device_id={"row": dest}, device_id_type=MESH)
        return carry

    def greet_col(k, carry):
        dest = lax.rem(col + 1 + k, NC)
        pl.semaphore_signal(barrier, inc=1, device_id={"col": dest}, device_id_type=MESH)
        return carry

    lax.fori_loop(0, NR - 1, greet, 0)
    lax.fori_loop(0, NC - 1, greet_col, 0)

    def send_all(src, dst, ssem, rsem, axis, me, n, first, last):
        tiles = pl.ds(first, last - first)

        def one(k, carry):
            dest = lax.rem(me + peer_step(k, n), n)
            pltpu.make_async_remote_copy(
                src.at[dest, tiles], dst.at[me, tiles], ssem, rsem, device_id={axis: dest}, device_id_type=MESH
            ).start()
            return carry

        lax.fori_loop(0, n - 1, one, 0)
        dst[me, first:last] = src[me, first:last]

    def wait_all(buffer, sem, n, first, last):
        part = buffer.at[pl.ds(0, n - 1), pl.ds(first, last - first)]
        pltpu.make_async_copy(part, part, sem).wait()

    loads[0].wait()
    loads[1].wait()
    scale = gn[...].astype(F32).reshape(1, D)

    def norm(n, carry):
        x = xb[pl.ds(2 * n, 2)].astype(F32).reshape(16, D)
        y = x * lax.rsqrt(jnp.mean(x * x, axis=-1, keepdims=True) + NORM_EPS) * scale
        xs[pl.ds(pl.multiple_of(16 * n, 16), 16), :] = y.astype(BF16)
        return carry

    lax.fori_loop(0, 9, norm, 0)
    loads[2].wait()
    loads[3].wait()
    mp[...] = jnp.dot(xs[...], wi[...], preferred_element_type=F32).astype(BF16)
    for g in range(GROUPS):
        o, t = g // 3, g % 3
        values = jnp.dot(mp[:, 128 * g : 128 * (g + 1)], tc[...], preferred_element_type=F32)
        tb[t, :, 8 * o : 8 * (o + 1), :] = values.reshape(18, 8, GROUP)

    def place(moved, tile):
        for q in range(8):
            for o in range(3):
                s1[8 * o + q, tile] = moved[q][8 * o : 8 * (o + 1)].astype(BF16)

    for t in range(3):
        first, last = TILES1[t]
        for hi in range(2):
            place(swap8([tb[t, 8 * hi + n] for n in range(8)]), first + hi)
        if t == 0:
            zero = jnp.zeros((24, GROUP), F32)
            place(swap8([tb[n % 4, 16 + n // 4] if n % 4 < 3 else zero for n in range(8)]), 2)
            pl.semaphore_wait(barrier, NR + NC - 2)
        send_all(s1, r1, send1.at[t], recv1.at[t], "row", row, NR, first, last)

    shape = (LEN_B, GROUP)
    line = lax.broadcasted_iota(jnp.int32, shape, 0)
    lane = lax.broadcasted_iota(jnp.int32, shape, 1)
    position = (18 * (line & 31) + (line >> 5)).astype(F32)
    sine = ((lane & 8) != 0) & jnp.logical_not((lax.rem(row, 8) == 0) & ((lane & 15) == 8))
    offset = jnp.where(sine, 0.5 * math.pi, 0.0).astype(F32)
    i = lane >> 4
    frequency = jnp.where(i < 3, 3 * col + i, LEN_A - (3 * col + i - 3))
    frequency = jnp.where((i == 3) & (col == 0), LEN_A // 2, frequency).astype(F32)
    angle = position * frequency * (2.0 * math.pi / POSITIONS) + offset
    cs[...] = jnp.cos(angle)
    sn[...] = jnp.sin(angle)
    loads[4].wait()
    za[pl.ds(3, 8 * NC, stride=4), :] = jnp.zeros((8 * NC, GROUP), F32)
    for n in (54, 55):
        m3[pl.ds(n, NR, stride=56), :] = jnp.zeros((NR, GROUP), F32)

    for t in range(3):
        first, last = TILES1[t]
        wait_all(r1, recv1.at[t], NR, first, last)
        arrived = [r1[:, n].astype(F32).reshape(LEN_A, GROUP) for n in range(first, last)]
        arrived = jnp.concatenate(arrived, axis=1).astype(BF16)
        turned = jnp.dot(ma[...], arrived, preferred_element_type=F32)
        if t == 0:
            for n in range(3):
                za[pl.ds(n, 8 * NC, stride=4), :] = turned[:, 128 * n : 128 * (n + 1)]
            sa[...] = za[...].reshape(NC, 4, 8, GROUP).astype(BF16)
            send_all(sa, ra, send2.at[t], recv2.at[t], "col", col, NC, 0, 3)
        else:
            for n in range(2):
                zb[pl.ds(n, 8 * NC, stride=2), :] = turned[:, 128 * n : 128 * (n + 1)]
            sb[t - 1] = zb[...].reshape(NC, 2, 8, GROUP).astype(BF16)
            send_all(sb.at[t - 1], rb.at[t - 1], send2.at[t], recv2.at[t], "col", col, NC, 0, 2)

    loads[5].wait()
    loads[6].wait()
    for t in range(3):
        for o in range(3):
            source, target = 128 * (3 * o + t), 128 * (3 * t + o)
            wf[target : target + 128, :] = jnp.dot(
                fold[...], wo[source : source + 128, :], preferred_element_type=F32
            ).astype(BF16)
    loads[7].wait()

    inner = (col != 0).astype(F32)
    zero = jnp.zeros((NC, GROUP), F32)

    def spread(part):
        r0, r1_, r2_, i0, i1, i2 = [part(n) for n in range(6)]
        mirrored = jnp.where(col == 0, i0, r0)
        i0 = i0 * inner
        real = swap8([r0, r1_, r2_, mirrored, r1_, r2_, zero, zero])
        imag = swap8([i0, i1, i2, -i0, -i1, -i2, zero, zero])
        return real, imag

    for t in range(3):
        if t == 0:
            wait_all(ra, recv2.at[t], NC, 0, 3)
            fa[...] = ra[...].astype(F32).reshape(NC * 24, GROUP)
            real, imag = spread(lambda n: fa[pl.ds(4 * n + 2, NC, stride=24), :])
            for b2 in range(2):
                at = slice(32 * (16 + b2), 32 * (17 + b2))
                for u in range(3):
                    rr[u, at, :] = real[4 * b2 + u]
                    ii[u, at, :] = imag[4 * b2 + u]
        else:
            wait_all(rb.at[t - 1], recv2.at[t], NC, 0, 2)
            fb[...] = rb[t - 1].astype(F32).reshape(NC * 16, GROUP)
        for hi in range(2):
            if t == 0:
                real, imag = spread(lambda n: fa[pl.ds(4 * n + hi, NC, stride=24), :])
            else:
                real, imag = spread(lambda n: fb[pl.ds(2 * n + hi, NC, stride=16), :])
            for n in range(8):
                at = slice(32 * (8 * hi + n), 32 * (8 * hi + n + 1))
                rr[t, at, :] = real[n]
                ii[t, at, :] = imag[n]
        dd[0:LEN_B, :] = (rr[t] * cs[...] + ii[t] * sn[...]).astype(BF16)
        dd[LEN_B : 2 * LEN_B, :] = (ii[t] * cs[...] - rr[t] * sn[...]).astype(BF16)
        result = jnp.dot(gg[...], dd[...], preferred_element_type=F32)
        moved = swap8([result[72 * n : 72 * (n + 1)] for n in range(8)])
        for i in range(6):
            for hi in range(3):
                m3[pl.ds(18 * t + 3 * i + hi, NR, stride=56), :] = moved[i][24 * hi : 24 * (hi + 1)]
        first, last = TILES3[t]
        s3[:, first:last] = m3.reshape(NR, 7, 8, GROUP)[:, first:last].astype(BF16)
        send_all(s3, r3, send3.at[t], recv3.at[t], "row", row, NR, first, last)

    def take(first, last):
        f3.reshape(NR, 7, 8, GROUP)[:, first:last] = r3[:, first:last].astype(F32)

    def project(t, last):
        for o in range(3):
            moved = swap8([f3[pl.ds((8 * o + q) * 56 + 18 * t, 18), :] for q in range(8)])
            for n in range(8):
                lh[o, pl.ds(n, 18, stride=8), :] = moved[n]
        values = jnp.concatenate([lh[o] for o in range(3)], axis=1).astype(BF16)
        for n in range(D // 512):
            at = slice(512 * n, 512 * (n + 1))
            part = jnp.dot(values, wf[384 * t : 384 * (t + 1), at], preferred_element_type=F32)
            if t:
                part = part + acc[:, at]
            if last:
                out[:, at] = part.astype(BF16)
            else:
                acc[:, at] = part

    wait_all(r3, recv3.at[0], NR, *TILES3[0])
    wait_all(r3, recv3.at[1], NR, *TILES3[1])
    take(0, 4)
    project(0, False)
    wait_all(r3, recv3.at[2], NR, *TILES3[2])
    take(4, 7)
    project(1, False)
    project(2, True)

    for t in range(3):
        wait_all(s1, send1.at[t], NR, *TILES1[t])
        if t == 0:
            wait_all(sa, send2.at[t], NC, 0, 3)
        else:
            wait_all(sb.at[t - 1], send2.at[t], NC, 0, 2)
        wait_all(s3, send3.at[t], NR, *TILES3[t])


def shards(tokens, norm_gain, w_in, w_out):
    vm = pltpu.VMEM
    dma = pltpu.SemaphoreType.DMA
    out = pl.pallas_call(
        kernel,
        out_shape=jax.ShapeDtypeStruct((144, D), BF16),
        in_specs=[pl.BlockSpec(memory_space=pl.ANY)] * 8,
        out_specs=pl.BlockSpec(memory_space=vm),
        scratch_shapes=[
            vm((18, 8, D), BF16),
            vm((D,), BF16),
            vm((144, D), BF16),
            vm((D, F), BF16),
            vm((F, D), BF16),
            vm((F, D), BF16),
            vm((GROUP, GROUP), BF16),
            vm((8 * NC, LEN_A), BF16),
            vm((LEN_B, 2 * LEN_B), BF16),
            vm((GROUP, GROUP), BF16),
            vm((144, F), BF16),
            vm((3, 18, 24, GROUP), F32),
            vm((NR, 7, 8, GROUP), BF16),
            vm((NR, 7, 8, GROUP), BF16),
            vm((NC * 32, GROUP), F32),
            vm((NC * 16, GROUP), F32),
            vm((NC, 4, 8, GROUP), BF16),
            vm((NC, 3, 8, GROUP), BF16),
            vm((2, NC, 2, 8, GROUP), BF16),
            vm((2, NC, 2, 8, GROUP), BF16),
            vm((NC * 24, GROUP), F32),
            vm((NC * 16, GROUP), F32),
            vm((3, LEN_B, GROUP), F32),
            vm((3, LEN_B, GROUP), F32),
            vm((LEN_B, GROUP), F32),
            vm((LEN_B, GROUP), F32),
            vm((2 * LEN_B, GROUP), BF16),
            vm((NR * 56, GROUP), F32),
            vm((NR, 7, 8, GROUP), BF16),
            vm((NR, 7, 8, GROUP), BF16),
            vm((NR * 56, GROUP), F32),
            vm((3, 144, GROUP), F32),
            vm((144, D), F32),
            dma((8,)),
            dma((3,)),
            dma((3,)),
            dma((3,)),
            dma((3,)),
            dma((3,)),
            dma((3,)),
        ],
        compiler_params=pltpu.CompilerParams(
            collective_id=0, has_side_effects=True, vmem_limit_bytes=60 * 1024 * 1024
        ),
    )(tokens.transpose(1, 0, 2), norm_gain, w_in, w_out, *[jnp.asarray(t) for t in TABLES])
    return out.reshape(6, 3, 8, D).transpose(1, 2, 0, 3).reshape(24, 6, D)


def solution(mesh):
    in_specs = (P("row", "col", None), P(), P(), P())
    out_specs = P("row", "col", None)
    return jax.shard_map(shards, mesh=mesh, in_specs=in_specs, out_specs=out_specs, check_vma=False)
```

time: 73.9 us -> 57.7 us (0.78)
  Pallas kernels: 68.1 us -> 55.6 us
  local copies, waits for them, and re-layouts: 5.51 us -> 1.93 us
    pallas_call x1, Pallas kernels: 68.1 us -> 55.6 us  [shards(): pl.pallas_call(kernel, out_shape=jax.ShapeDtypeStruct((144, D), BF16), in...]
    unnamed x2 -> x1, local copies, waits for them, and re-layouts: 4.22 us -> 1.93 us
    reshape x1 -> x0, local copies, waits for them, and re-layouts: 1.29 us -> none  [shards(): norm_gain.reshape(1, D)]
where the time goes in v1:
time: 57.7 us; the launch traced here: 57.5 us
  Pallas kernels  55.6 us (96%)
  local copies, waits for them, and re-layouts  1.93 us (3%)
    pallas_call x1, Pallas kernels, shards(): pl.pallas_call(kernel, out_shape=jax.ShapeDtypeStruct((144, D), BF16), in...  55.6 us
    unnamed x1, local copies, waits for them, and re-layouts  1.93 us

profile of v1, /device:TPU:1, one launch (start us, length us, event | category | flops | bytes accessed | tf_op | source)
XLA Modules:
  0.0 57.5 jit_solution(2742198632201306342)
XLA Ops:
  0.0 55.6 %shard_map.82 = bf16[144,2048]{1,0:T(8,128)(2,1)} custom-call(bf16[18,8,2048]{2,1,0:T(8,128)(2,1)} %bitcast.7, bf16[2048]{0:T(1024)(128)(2,1)} %gain.1, bf16[2048,1152]{1,0:T(8,128)(2,1)} %w_in.1, bf16[1152,2048]{1,0:T(8,128)(2,1)} %w_out.1, bf16[128,128]{1,0:T(8,128)(2,1)} %constant.8.clone.tc_h, bf16[256,192]{1,0:T(8,128)(2,1)} %constant.9.clone.ma_h, ...), custom_call_target="tpu_custom_call" | custom-call | tf_op jit(solution)/shard_map/pallas_call | solution.py:291
  55.6 1.9 %copy.10 = bf16[24,6,2048]{2,0,1:T(8,128)(2,1)} copy(bf16[24,6,2048]{2,0,1:T(8,128)(2,1)} %bitcast.6) | data formatting | bytes 1179648

commit v2 on v1

--- a/solution.py
+++ b/solution.py
@@ -49,10 +49,14 @@
     b = (18 * cp + bp).reshape(-1)
     w = 2 * np.pi * (kb[:, None] * b[None, :] % LEN_B) / LEN_B
     g = np.concatenate([np.cos(w), np.sin(w)], axis=1) / math.sqrt(LEN_B)
-    return [np.asarray(t, dtype=jnp.bfloat16) for t in (tc, ma, g, fold)]
-
-
-TABLES = host_tables()
+    small = np.zeros((8 * NC, 2 * LEN_B))
+    small[:, :LEN_A] = ma
+    small[:GROUP, 256:384] = tc
+    small[:GROUP, 384:512] = fold
+    return np.asarray(np.concatenate([g, small]), dtype=jnp.bfloat16)
+
+
+TABLE = host_tables()
 TILES1 = ((0, 3), (3, 5), (5, 7))
 TILES3 = ((0, 2), (2, 4), (4, 7))
 
@@ -72,14 +76,9 @@
     return x
 
 
-def peer_step(k, n):
-    k = n - 2 - k
-    return jnp.where(k % 2 == 0, 1 + k // 2, n - (k + 1) // 2)
-
-
 def kernel(
-    tok, gain, w_in, w_out, tc_h, ma_h, g_h, fold_h, out,
-    xb, gn, xs, wi, wo, wf, tc, ma, gg, fold, mp, tb, s1, r1, za, zb, sa, ra, sb, rb, fa, fb,
+    tok, gain, w_in, w_out, table, out,
+    xb, gn, xs, wi, wo, wf, small, gg, ma, mp, tb, s1, r1, zr, zb, sb, rb, fb,
     rr, ii, cs, sn, dd, m3, s3, r3, f3, lh, acc,
     load_sem, send1, recv1, send2, recv2, send3, recv3,
 ):
@@ -88,38 +87,48 @@
     loads = [
         pltpu.make_async_copy(src, dst, load_sem.at[n])
         for n, (src, dst) in enumerate(
-            [(tok, xb), (gain, gn), (w_in, wi), (tc_h, tc), (ma_h, ma), (fold_h, fold), (w_out, wo), (g_h, gg)]
+            [
+                (tok, xb),
+                (gain, gn),
+                *[(w_in.at[pl.ds(512 * k, 512)], wi.at[pl.ds(512 * k, 512)]) for k in range(4)],
+                (table.at[LEN_B:, 0:512], small),
+                (table.at[0:LEN_B], gg),
+                (w_out, wo),
+            ]
         )
     ]
-    for load in loads:
+    for load in loads[:7]:
         load.start()
 
     barrier = pltpu.get_barrier_semaphore()
 
-    def greet(k, carry):
-        dest = lax.rem(row + 1 + k, NR)
-        pl.semaphore_signal(barrier, inc=1, device_id={"row": dest}, device_id_type=MESH)
-        return carry
-
-    def greet_col(k, carry):
-        dest = lax.rem(col + 1 + k, NC)
-        pl.semaphore_signal(barrier, inc=1, device_id={"col": dest}, device_id_type=MESH)
-        return carry
-
-    lax.fori_loop(0, NR - 1, greet, 0)
-    lax.fori_loop(0, NC - 1, greet_col, 0)
+    def both_ways(me, n, act):
+        act(jnp.where(me >= n // 2, me - n // 2, me + n // 2))
+
+        def one(k, carry):
+            d = n // 2 - 1 - k
+            up, down = me + d, me - d
+            act(jnp.where(up >= n, up - n, up))
+            act(jnp.where(down < 0, down + n, down))
+            return carry
+
+        lax.fori_loop(0, n // 2 - 1, one, 0)
+
+    def greet(axis):
+        return lambda peer: pl.semaphore_signal(barrier, inc=1, device_id={axis: peer}, device_id_type=MESH)
+
+    both_ways(row, NR, greet("row"))
+    both_ways(col, NC, greet("col"))
 
     def send_all(src, dst, ssem, rsem, axis, me, n, first, last):
         tiles = pl.ds(first, last - first)
 
-        def one(k, carry):
-            dest = lax.rem(me + peer_step(k, n), n)
+        def one(dest):
             pltpu.make_async_remote_copy(
                 src.at[dest, tiles], dst.at[me, tiles], ssem, rsem, device_id={axis: dest}, device_id_type=MESH
             ).start()
-            return carry
-
-        lax.fori_loop(0, n - 1, one, 0)
+
+        both_ways(me, n, one)
         dst[me, first:last] = src[me, first:last]
 
     def wait_all(buffer, sem, n, first, last):
@@ -136,13 +145,23 @@
         xs[pl.ds(pl.multiple_of(16 * n, 16), 16), :] = y.astype(BF16)
         return carry
 
-    lax.fori_loop(0, 9, norm, 0)
-    loads[2].wait()
-    loads[3].wait()
-    mp[...] = jnp.dot(xs[...], wi[...], preferred_element_type=F32).astype(BF16)
+    lax.fori_loop(0, 9, norm, 0, unroll=True)
+    for k in range(4):
+        at = slice(512 * k, 512 * (k + 1))
+        loads[2 + k].wait()
+        part = jnp.dot(xs[:, at], wi[at, :], preferred_element_type=F32)
+        if k:
+            part = part + ma[...]
+        if k < 3:
+            ma[...] = part
+        else:
+            mp[...] = part.astype(BF16)
+    loads[6].wait()
+    loads[7].start()
+    loads[8].start()
     for g in range(GROUPS):
         o, t = g // 3, g % 3
-        values = jnp.dot(mp[:, 128 * g : 128 * (g + 1)], tc[...], preferred_element_type=F32)
+        values = jnp.dot(mp[:, 128 * g : 128 * (g + 1)], small[0:GROUP, 256:384], preferred_element_type=F32)
         tb[t, :, 8 * o : 8 * (o + 1), :] = values.reshape(18, 8, GROUP)
 
     def place(moved, tile):
@@ -156,7 +175,7 @@
             place(swap8([tb[t, 8 * hi + n] for n in range(8)]), first + hi)
         if t == 0:
             zero = jnp.zeros((24, GROUP), F32)
-            place(swap8([tb[n % 4, 16 + n // 4] if n % 4 < 3 else zero for n in range(8)]), 2)
+            place(swap8([tb[n // 2, 16 + n % 2] if n < 6 else zero for n in range(8)]), 2)
             pl.semaphore_wait(barrier, NR + NC - 2)
         send_all(s1, r1, send1.at[t], recv1.at[t], "row", row, NR, first, last)
 
@@ -172,36 +191,32 @@
     angle = position * frequency * (2.0 * math.pi / POSITIONS) + offset
     cs[...] = jnp.cos(angle)
     sn[...] = jnp.sin(angle)
-    loads[4].wait()
-    za[pl.ds(3, 8 * NC, stride=4), :] = jnp.zeros((8 * NC, GROUP), F32)
     for n in (54, 55):
         m3[pl.ds(n, NR, stride=56), :] = jnp.zeros((NR, GROUP), F32)
+
+    def turn(x, shift):
+        return pltpu.roll(x, shift % GROUP, 1) if shift % GROUP else x
 
     for t in range(3):
         first, last = TILES1[t]
         wait_all(r1, recv1.at[t], NR, first, last)
         arrived = [r1[:, n].astype(F32).reshape(LEN_A, GROUP) for n in range(first, last)]
         arrived = jnp.concatenate(arrived, axis=1).astype(BF16)
-        turned = jnp.dot(ma[...], arrived, preferred_element_type=F32)
+        turned = jnp.dot(small[:, 0:LEN_A], arrived, preferred_element_type=F32)
+        for n in range(2):
+            zb[pl.ds(n, 8 * NC, stride=2), :] = turned[:, 128 * n : 128 * (n + 1)]
         if t == 0:
-            for n in range(3):
-                za[pl.ds(n, 8 * NC, stride=4), :] = turned[:, 128 * n : 128 * (n + 1)]
-            sa[...] = za[...].reshape(NC, 4, 8, GROUP).astype(BF16)
-            send_all(sa, ra, send2.at[t], recv2.at[t], "col", col, NC, 0, 3)
-        else:
-            for n in range(2):
-                zb[pl.ds(n, 8 * NC, stride=2), :] = turned[:, 128 * n : 128 * (n + 1)]
-            sb[t - 1] = zb[...].reshape(NC, 2, 8, GROUP).astype(BF16)
-            send_all(sb.at[t - 1], rb.at[t - 1], send2.at[t], recv2.at[t], "col", col, NC, 0, 2)
-
-    loads[5].wait()
-    loads[6].wait()
-    for t in range(3):
-        for o in range(3):
-            source, target = 128 * (3 * o + t), 128 * (3 * t + o)
-            wf[target : target + 128, :] = jnp.dot(
-                fold[...], wo[source : source + 128, :], preferred_element_type=F32
-            ).astype(BF16)
+            zr[...] = turned[:, 256:384]
+        left = [zr[pl.ds(n, NC, stride=8), :] for n in range(6)]
+        block = lax.broadcasted_iota(jnp.int32, (NC, GROUP), 1) >> 5
+        for half, slots in ((0, (0, 1, 2, 3)), (1, (4, 5))):
+            line = jnp.zeros((NC, GROUP), F32)
+            for n in slots:
+                line = jnp.where(block == n % 4, turn(left[n], 32 * (n % 4 - t)), line)
+            zb[pl.ds(12 + half, NC, stride=16), :] = line
+        sb[t] = zb[...].reshape(NC, 2, 8, GROUP).astype(BF16)
+        send_all(sb.at[t], rb.at[t], send2.at[t], recv2.at[t], "col", col, NC, 0, 2)
+
     loads[7].wait()
 
     inner = (col != 0).astype(F32)
@@ -215,24 +230,30 @@
         imag = swap8([i0, i1, i2, -i0, -i1, -i2, zero, zero])
         return real, imag
 
-    for t in range(3):
-        if t == 0:
-            wait_all(ra, recv2.at[t], NC, 0, 3)
-            fa[...] = ra[...].astype(F32).reshape(NC * 24, GROUP)
-            real, imag = spread(lambda n: fa[pl.ds(4 * n + 2, NC, stride=24), :])
-            for b2 in range(2):
-                at = slice(32 * (16 + b2), 32 * (17 + b2))
-                for u in range(3):
-                    rr[u, at, :] = real[4 * b2 + u]
-                    ii[u, at, :] = imag[4 * b2 + u]
-        else:
-            wait_all(rb.at[t - 1], recv2.at[t], NC, 0, 2)
-            fb[...] = rb[t - 1].astype(F32).reshape(NC * 16, GROUP)
+    granule = lax.broadcasted_iota(jnp.int32, (NC, GROUP), 1) >> 4
+
+    def gather(picks):
+        tile = zero
+        for n, (x, k, f) in enumerate(picks):
+            value = turn(x, 16 * (n - k))
+            tile = jnp.where(granule == n, value if f is None else value * f, tile)
+        return tile
+
+    for t in range(3):
+        wait_all(rb.at[t], recv2.at[t], NC, 0, 2)
+        fb[...] = rb[t].astype(F32).reshape(NC * 16, GROUP)
+        x, y = fb[pl.ds(12, NC, stride=16), :], fb[pl.ds(13, NC, stride=16), :]
+        for b2 in range(2):
+            at = slice(32 * (16 + b2), 32 * (17 + b2))
+            i0, i1, i2 = (x, 6 + b2), (y, b2), (y, 2 + b2)
+            r0, r1_, r2_ = [(x, 2 * n + b2, None) for n in range(3)]
+            tile = gather([r0, r1_, r2_, r0, r1_, r2_])
+            rr[t, at, :] = jnp.where((granule == 3) & (col == 0), turn(x, 16 * (3 - i0[1])), tile)
+            ii[t, at, :] = gather(
+                [(*i0, inner), (*i1, None), (*i2, None), (*i0, -inner), (*i1, -1.0), (*i2, -1.0)]
+            )
         for hi in range(2):
-            if t == 0:
-                real, imag = spread(lambda n: fa[pl.ds(4 * n + hi, NC, stride=24), :])
-            else:
-                real, imag = spread(lambda n: fb[pl.ds(2 * n + hi, NC, stride=16), :])
+            real, imag = spread(lambda n: fb[pl.ds(2 * n + hi, NC, stride=16), :])
             for n in range(8):
                 at = slice(32 * (8 * hi + n), 32 * (8 * hi + n + 1))
                 rr[t, at, :] = real[n]
@@ -267,6 +288,13 @@
             else:
                 acc[:, at] = part
 
+    loads[8].wait()
+    for t in range(3):
+        for o in range(3):
+            source, target = 128 * (3 * o + t), 128 * (3 * t + o)
+            wf[target : target + 128, :] = jnp.dot(
+                small[0:GROUP, 384:512], wo[source : source + 128, :], preferred_element_type=F32
+            ).astype(BF16)
     wait_all(r3, recv3.at[0], NR, *TILES3[0])
     wait_all(r3, recv3.at[1], NR, *TILES3[1])
     take(0, 4)
@@ -278,20 +306,18 @@
 
     for t in range(3):
         wait_all(s1, send1.at[t], NR, *TILES1[t])
-        if t == 0:
-            wait_all(sa, send2.at[t], NC, 0, 3)
-        else:
-            wait_all(sb.at[t - 1], send2.at[t], NC, 0, 2)
+        wait_all(sb.at[t], send2.at[t], NC, 0, 2)
         wait_all(s3, send3.at[t], NR, *TILES3[t])
 
 
 def shards(tokens, norm_gain, w_in, w_out):
     vm = pltpu.VMEM
     dma = pltpu.SemaphoreType.DMA
+    operands = tokens.transpose(1, 0, 2), norm_gain, w_in, w_out, jnp.asarray(TABLE)
     out = pl.pallas_call(
         kernel,
         out_shape=jax.ShapeDtypeStruct((144, D), BF16),
-        in_specs=[pl.BlockSpec(memory_space=pl.ANY)] * 8,
+        in_specs=[pl.BlockSpec(memory_space=pl.ANY)] * 5,
         out_specs=pl.BlockSpec(memory_space=vm),
         scratch_shapes=[
             vm((18, 8, D), BF16),
@@ -300,21 +326,17 @@
             vm((D, F), BF16),
             vm((F, D), BF16),
             vm((F, D), BF16),
-            vm((GROUP, GROUP), BF16),
-            vm((8 * NC, LEN_A), BF16),
+            vm((8 * NC, 512), BF16),
             vm((LEN_B, 2 * LEN_B), BF16),
-            vm((GROUP, GROUP), BF16),
+            vm((144, F), F32),
             vm((144, F), BF16),
             vm((3, 18, 24, GROUP), F32),
             vm((NR, 7, 8, GROUP), BF16),
             vm((NR, 7, 8, GROUP), BF16),
-            vm((NC * 32, GROUP), F32),
+            vm((NC * 8, GROUP), F32),
             vm((NC * 16, GROUP), F32),
-            vm((NC, 4, 8, GROUP), BF16),
-            vm((NC, 3, 8, GROUP), BF16),
-            vm((2, NC, 2, 8, GROUP), BF16),
-            vm((2, NC, 2, 8, GROUP), BF16),
-            vm((NC * 24, GROUP), F32),
+            vm((3, NC, 2, 8, GROUP), BF16),
+            vm((3, NC, 2, 8, GROUP), BF16),
             vm((NC * 16, GROUP), F32),
             vm((3, LEN_B, GROUP), F32),
             vm((3, LEN_B, GROUP), F32),
@@ -327,7 +349,7 @@
             vm((NR * 56, GROUP), F32),
             vm((3, 144, GROUP), F32),
             vm((144, D), F32),
-            dma((8,)),
+            dma((9,)),
             dma((3,)),
             dma((3,)),
             dma((3,)),
@@ -336,9 +358,9 @@
             dma((3,)),
         ],
         compiler_params=pltpu.CompilerParams(
-            collective_id=0, has_side_effects=True, vmem_limit_bytes=60 * 1024 * 1024
+            collective_id=0, has_side_effects=True, vmem_limit_bytes=50 * 1024 * 1024
         ),
-    )(tokens.transpose(1, 0, 2), norm_gain, w_in, w_out, *[jnp.asarray(t) for t in TABLES])
+    )(*[pltpu.with_memory_space_constraint(x, pltpu.HBM) for x in operands])
     return out.reshape(6, 3, 8, D).transpose(1, 2, 0, 3).reshape(24, 6, D)
 
 

time: 57.7 us -> 53 us (0.919)
  Pallas kernels: 55.6 us -> 52 us
  local copies, waits for them, and re-layouts: 1.93 us -> 0.82 us
    pallas_call x1, Pallas kernels: 55.6 us -> 52 us  [shards(): pl.pallas_call(kernel, out_shape=jax.ShapeDtypeStruct((144, D), BF16), in...]
    unnamed x1, local copies, waits for them, and re-layouts: 1.93 us -> 0.82 us
where the time goes in v2:
time: 53 us; the launch traced here: 52.9 us
  Pallas kernels  52 us (98%)
  local copies, waits for them, and re-layouts  0.82 us (2%)
    pallas_call x1, Pallas kernels, shards(): pl.pallas_call(kernel, out_shape=jax.ShapeDtypeStruct((144, D), BF16), in...  52 us

profile of v2, /device:TPU:1, one launch (start us, length us, event | category | flops | bytes accessed | tf_op | source)
XLA Modules:
  0.0 52.9 jit_solution(1443822079244158955)
XLA Ops:
  0.0 52.0 %shard_map.55 = bf16[144,2048]{1,0:T(8,128)(2,1)S(1)} custom-call(bf16[18,8,2048]{2,1,0:T(8,128)(2,1)} %bitcast.7, bf16[2048]{0:T(1024)(128)(2,1)} %gain.1, bf16[2048,1152]{1,0:T(8,128)(2,1)} %w_in.1, bf16[1152,2048]{1,0:T(8,128)(2,1)} %w_out.1, bf16[832,1152]{1,0:T(8,128)(2,1)} %constant.2.clone.table), custom_call_target="tpu_custom_call" | custom-call | tf_op jit(solution)/shard_map/pallas_call | solution.py:317
  52.1 0.8 %copy.7 = bf16[24,6,2048]{2,0,1:T(8,128)(2,1)} copy(bf16[24,6,2048]{2,0,1:T(8,128)(2,1)S(1)} %bitcast.6) | data formatting | bytes 1179648

commit v3 on v2

--- a/solution.py
+++ b/solution.py
@@ -71,8 +71,11 @@
             if i & s:
                 continue
             a, b = x[i], x[i + s]
-            x[i] = jnp.where(bit, pltpu.roll(b, shift, 1), a)
-            x[i + s] = jnp.where(bit, b, pltpu.roll(a, GROUP - shift, 1))
+            turned = pltpu.roll(a, GROUP - shift, 1)
+            if b is None:
+                x[i], x[i + s] = jnp.where(bit, 0.0, a), jnp.where(bit, 0.0, turned)
+            else:
+                x[i], x[i + s] = jnp.where(bit, pltpu.roll(b, shift, 1), a), jnp.where(bit, b, turned)
     return x
 
 
@@ -90,14 +93,14 @@
             [
                 (tok, xb),
                 (gain, gn),
-                *[(w_in.at[pl.ds(512 * k, 512)], wi.at[pl.ds(512 * k, 512)]) for k in range(4)],
+                *[(w_in.at[pl.ds(256 * k, 256)], wi.at[pl.ds(256 * k, 256)]) for k in range(8)],
                 (table.at[LEN_B:, 0:512], small),
                 (table.at[0:LEN_B], gg),
                 (w_out, wo),
             ]
         )
     ]
-    for load in loads[:7]:
+    for load in loads[:11]:
         load.start()
 
     barrier = pltpu.get_barrier_semaphore()
@@ -148,7 +151,8 @@
     lax.fori_loop(0, 9, norm, 0, unroll=True)
     for k in range(4):
         at = slice(512 * k, 512 * (k + 1))
-        loads[2 + k].wait()
+        loads[2 + 2 * k].wait()
+        loads[3 + 2 * k].wait()
         part = jnp.dot(xs[:, at], wi[at, :], preferred_element_type=F32)
         if k:
             part = part + ma[...]
@@ -156,9 +160,9 @@
             ma[...] = part
         else:
             mp[...] = part.astype(BF16)
-    loads[6].wait()
-    loads[7].start()
-    loads[8].start()
+    loads[10].wait()
+    loads[11].start()
+    loads[12].start()
     for g in range(GROUPS):
         o, t = g // 3, g % 3
         values = jnp.dot(mp[:, 128 * g : 128 * (g + 1)], small[0:GROUP, 256:384], preferred_element_type=F32)
@@ -174,8 +178,7 @@
         for hi in range(2):
             place(swap8([tb[t, 8 * hi + n] for n in range(8)]), first + hi)
         if t == 0:
-            zero = jnp.zeros((24, GROUP), F32)
-            place(swap8([tb[n // 2, 16 + n % 2] if n < 6 else zero for n in range(8)]), 2)
+            place(swap8([tb[n // 2, 16 + n % 2] if n < 6 else None for n in range(8)]), 2)
             pl.semaphore_wait(barrier, NR + NC - 2)
         send_all(s1, r1, send1.at[t], recv1.at[t], "row", row, NR, first, last)
 
@@ -217,7 +220,7 @@
         sb[t] = zb[...].reshape(NC, 2, 8, GROUP).astype(BF16)
         send_all(sb.at[t], rb.at[t], send2.at[t], recv2.at[t], "col", col, NC, 0, 2)
 
-    loads[7].wait()
+    loads[11].wait()
 
     inner = (col != 0).astype(F32)
     zero = jnp.zeros((NC, GROUP), F32)
@@ -226,8 +229,8 @@
         r0, r1_, r2_, i0, i1, i2 = [part(n) for n in range(6)]
         mirrored = jnp.where(col == 0, i0, r0)
         i0 = i0 * inner
-        real = swap8([r0, r1_, r2_, mirrored, r1_, r2_, zero, zero])
-        imag = swap8([i0, i1, i2, -i0, -i1, -i2, zero, zero])
+        real = swap8([r0, r1_, r2_, mirrored, r1_, r2_, None, None])
+        imag = swap8([i0, i1, i2, -i0, -i1, -i2, None, None])
         return real, imag
 
     granule = lax.broadcasted_iota(jnp.int32, (NC, GROUP), 1) >> 4
@@ -272,23 +275,25 @@
     def take(first, last):
         f3.reshape(NR, 7, 8, GROUP)[:, first:last] = r3[:, first:last].astype(F32)
 
-    def project(t, last):
-        for o in range(3):
-            moved = swap8([f3[pl.ds((8 * o + q) * 56 + 18 * t, 18), :] for q in range(8)])
-            for n in range(8):
-                lh[o, pl.ds(n, 18, stride=8), :] = moved[n]
-        values = jnp.concatenate([lh[o] for o in range(3)], axis=1).astype(BF16)
+    def project(chunks):
+        values = []
+        for t in chunks:
+            for o in range(3):
+                moved = swap8([f3[pl.ds((8 * o + q) * 56 + 18 * t, 18), :] for q in range(8)])
+                for n in range(8):
+                    lh[3 * t + o, pl.ds(n, 18, stride=8), :] = moved[n]
+                values.append(lh[3 * t + o])
+        values = jnp.concatenate(values, axis=1).astype(BF16)
+        lines = slice(384 * chunks[0], 384 * (chunks[-1] + 1))
         for n in range(D // 512):
             at = slice(512 * n, 512 * (n + 1))
-            part = jnp.dot(values, wf[384 * t : 384 * (t + 1), at], preferred_element_type=F32)
-            if t:
-                part = part + acc[:, at]
-            if last:
-                out[:, at] = part.astype(BF16)
+            part = jnp.dot(values, wf[lines, at], preferred_element_type=F32)
+            if chunks[0]:
+                out[:, at] = (part + acc[:, at]).astype(BF16)
             else:
                 acc[:, at] = part
 
-    loads[8].wait()
+    loads[12].wait()
     for t in range(3):
         for o in range(3):
             source, target = 128 * (3 * o + t), 128 * (3 * t + o)
@@ -298,11 +303,10 @@
     wait_all(r3, recv3.at[0], NR, *TILES3[0])
     wait_all(r3, recv3.at[1], NR, *TILES3[1])
     take(0, 4)
-    project(0, False)
+    project((0,))
     wait_all(r3, recv3.at[2], NR, *TILES3[2])
     take(4, 7)
-    project(1, False)
-    project(2, True)
+    project((1, 2))
 
     for t in range(3):
         wait_all(s1, send1.at[t], NR, *TILES1[t])
@@ -347,9 +351,9 @@
             vm((NR, 7, 8, GROUP), BF16),
             vm((NR, 7, 8, GROUP), BF16),
             vm((NR * 56, GROUP), F32),
-            vm((3, 144, GROUP), F32),
+            vm((9, 144, GROUP), F32),
             vm((144, D), F32),
-            dma((9,)),
+            dma((13,)),
             dma((3,)),
             dma((3,)),
             dma((3,)),

time: 53 us -> 53.1 us (level)
  no operation moved by 1% of the time
where the time goes in v3:
time: 53.1 us; the launch traced here: 52.9 us
  Pallas kernels  52.1 us (98%)
  local copies, waits for them, and re-layouts  0.82 us (2%)
    pallas_call x1, Pallas kernels, shards(): pl.pallas_call(kernel, out_shape=jax.ShapeDtypeStruct((144, D), BF16), in...  52.1 us

profile of v3, /device:TPU:1, one launch (start us, length us, event | category | flops | bytes accessed | tf_op | source)
XLA Modules:
  0.0 52.9 jit_solution(16563044229808297804)
XLA Ops:
  0.0 52.1 %shard_map.55 = bf16[144,2048]{1,0:T(8,128)(2,1)S(1)} custom-call(bf16[18,8,2048]{2,1,0:T(8,128)(2,1)} %bitcast.7, bf16[2048]{0:T(1024)(128)(2,1)} %gain.1, bf16[2048,1152]{1,0:T(8,128)(2,1)} %w_in.1, bf16[1152,2048]{1,0:T(8,128)(2,1)} %w_out.1, bf16[832,1152]{1,0:T(8,128)(2,1)} %constant.2.clone.table), custom_call_target="tpu_custom_call" | custom-call | tf_op jit(solution)/shard_map/pallas_call | solution.py:321
  52.1 0.8 %copy.7 = bf16[24,6,2048]{2,0,1:T(8,128)(2,1)} copy(bf16[24,6,2048]{2,0,1:T(8,128)(2,1)S(1)} %bitcast.6) | data formatting | bytes 1179648
